TPU v7x, 32 devices: a whole 2x2x4 slice. The times are simulated.
32 devices in a mesh: ep: 16 (over z, y, x), tp: 2 (over core).
Axes of the slice: x: 2, y: 2, z: 4, core: 2. Of those that a mesh axis runs over, the one named last changes fastest.
Arguments:
- tokens: bfloat16 [384, 2048], P('ep'), may hold values from -6 to 6
- norm_gain: bfloat16 [2048], replicated, may hold values from 0.099609375 to 1.8984375
- query_w: bfloat16 [2048, 1024], P(None, 'tp'), may hold values from -0.125 to 0.125
- key_w: bfloat16 [2048, 128], replicated, may hold values from -0.125 to 0.125
- value_w: bfloat16 [2048, 128], replicated, may hold values from -0.125 to 0.125
- forget_w: bfloat16 [2048, 16], replicated, may hold values from -0.125 to 0.125
- forget_bias: float32 [16], replicated, may hold values from 0 to 4
- query_gain: bfloat16 [64], replicated, may hold values from 0.099609375 to 1.8984375
- key_gain: bfloat16 [64], replicated, may hold values from 0.099609375 to 1.8984375
- cache_key: bfloat16 [384, 2, 64, 1024], P('ep', 'tp'), may hold values from -6 to 6
- cache_value: bfloat16 [384, 2, 64, 1024], P('ep', 'tp'), may hold values from -6 to 6
- cache_gate: float32 [384, 16, 1024], P('ep', 'tp'), may hold values from -105 to 0, as said below
- cache_len: int32 [384], P('ep'), may hold values from 256 to 1024
- out_w: bfloat16 [1024, 2048], P('tp'), may hold values from -0.1875 to 0.1875
- post_gain: bfloat16 [2048], replicated, may hold values from 0.099609375 to 1.8984375
- branch_gate: bfloat16 [2048], replicated, may hold values from -0.125 to 0.125
- dense_gate_w: bfloat16 [2048, 16384], P(None, ('ep', 'tp')), may hold values from -0.125 to 0.125
- dense_up_w: bfloat16 [2048, 16384], P(None, ('ep', 'tp')), may hold values from -1.3258252 to 1.3258252
- dense_down_w: bfloat16 [16384, 2048], P(('ep', 'tp')), may hold values from -0.046875 to 0.046875
- expert_choice: int32 [384, 2], P('ep'), may hold values from 0 to 15, as said below
- route_weight: float32 [384, 2], P('ep'), may hold values from 0.1 to 1
- expert_gate_w: bfloat16 [16, 2048, 1024], P('ep', None, 'tp'), may hold values from -0.125 to 0.125
- expert_up_w: bfloat16 [16, 2048, 1024], P('ep', None, 'tp'), may hold values from -0.125 to 0.125
- expert_down_w: bfloat16 [16, 1024, 2048], P('ep', 'tp'), may hold values from -0.1875 to 0.1875
Outputs:
- mixed_out: bfloat16 [384, 2048], P('ep', 'tp')
- fresh_key: bfloat16 [384, 2, 64], P('ep', 'tp')
- fresh_value: bfloat16 [384, 2, 64], P('ep', 'tp')
- fresh_gate: float32 [384, 16], P('ep', 'tp')
Inputs may be any that keep to these rules, and one draw needn't show every extreme that they name: `cache_gate`: Non-increasing along positions. `expert_choice`: experts 4 * g to 4 * g + 3 form group g. A token names 2 different experts of one group. Among the 24 tokens of one index of ep, those at even offsets all choose one group and the others choose other groups; no expert is named more than 6 times by them, and some expert exactly 6 times.
All inputs are finite; a program needn't handle non-finite values.
Results may differ from a plain program's by a relative error of at most 0.014.
Values may be sent and summed in bfloat16 or wider, within the bound.
A program may use at most 128 MiB of HBM per device.

v0:
```python
import jax
import jax.numpy as jnp
from jax import lax
from jax.sharding import PartitionSpec as P

FF2 = 16384
GROUPS = 4
norm_eps = 1e-06


def rms_scale(values, gain_vec):
    mean_square = jnp.mean(values * values, axis=-1, keepdims=True)
    return values * lax.rsqrt(mean_square + norm_eps) * gain_vec


def rounded(values):
    return lax.optimization_barrier(values.astype(jnp.bfloat16)).astype(jnp.float32)


def swiglu_rows(inputs, gate_weight, up_weight):
    gate_value = jnp.dot(inputs, gate_weight, preferred_element_type=jnp.float32)
    up_value = jnp.dot(inputs, up_weight, preferred_element_type=jnp.float32)
    return jax.nn.silu(gate_value) * up_value


def flat_terms(hidden, down_weight, ep_count, tp_count, seq_count):
    spread_hidden = hidden.astype(jnp.bfloat16).reshape(ep_count, seq_count, -1)
    split_down = down_weight.reshape(down_weight.shape[0], tp_count, -1)
    return jnp.einsum(
        "esh,hcd->ecsd", spread_hidden, split_down, preferred_element_type=jnp.float32
    )


def body(
    tokens,
    norm_gain,
    query_w,
    key_w,
    value_w,
    forget_w,
    forget_bias,
    query_gain,
    key_gain,
    cache_key,
    cache_value,
    cache_gate,
    cache_len,
    out_w,
    post_gain,
    branch_gate,
    dense_gate_w,
    dense_up_w,
    dense_down_w,
    expert_choice,
    route_weight,
    expert_gate_w,
    expert_up_w,
    expert_down_w,
):
    seq_count = tokens.shape[0]
    model_width = tokens.shape[1]
    heads_local = cache_gate.shape[1]
    kv_local = cache_key.shape[1]
    head_size = cache_key.shape[2]
    cache_span = cache_key.shape[3]
    tp_count = lax.axis_size("tp")
    ep_count = lax.axis_size("ep")
    tp_rank = lax.axis_index("tp")
    half_width = model_width // tp_count
    score_scale = head_size ** (-0.5)
    resid_in = tokens.astype(jnp.float32)
    normed = rms_scale(resid_in, norm_gain.astype(jnp.float32)).astype(jnp.bfloat16)
    queries = jnp.dot(normed, query_w, preferred_element_type=jnp.float32).reshape(
        seq_count, heads_local, head_size
    )
    queries = rms_scale(queries, query_gain.astype(jnp.float32)).astype(jnp.bfloat16)
    keys_all = jnp.dot(normed, key_w, preferred_element_type=jnp.float32).reshape(
        seq_count, -1, head_size
    )
    keys_all = rms_scale(keys_all, key_gain.astype(jnp.float32)).astype(jnp.bfloat16)
    values_all = (
        jnp.dot(normed, value_w, preferred_element_type=jnp.float32)
        .astype(jnp.bfloat16)
        .reshape(seq_count, -1, head_size)
    )
    fresh_key = lax.dynamic_slice_in_dim(keys_all, tp_rank * kv_local, kv_local, 1)
    fresh_value = lax.dynamic_slice_in_dim(values_all, tp_rank * kv_local, kv_local, 1)
    forget_all = jax.nn.log_sigmoid(
        jnp.dot(normed, forget_w, preferred_element_type=jnp.float32) + forget_bias
    )
    log_forget = lax.dynamic_slice_in_dim(forget_all, tp_rank * heads_local, heads_local, 1)
    repeat = heads_local // kv_local
    grouped = queries.reshape(seq_count, kv_local, repeat, head_size)
    scores = (
        jnp.einsum("sgrd,sgdl->sgrl", grouped, cache_key, preferred_element_type=jnp.float32)
        * score_scale
    )
    own_score = (
        jnp.einsum("sgrd,sgd->sgr", grouped, fresh_key, preferred_element_type=jnp.float32)
        * score_scale
    )
    current_slot_offset = lax.broadcasted_iota(jnp.int32, (seq_count, cache_span), 1)
    at_last = (current_slot_offset == cache_len[:, None] - 1)[:, None, :]
    previous = jnp.sum(jnp.where(at_last, cache_gate, jnp.zeros_like(cache_gate)), axis=2)
    current = previous + log_forget
    decay_bias = (current[:, :, None] - cache_gate).reshape(seq_count, kv_local, repeat, cache_span)
    is_valid = (current_slot_offset < cache_len[:, None])[:, None, None, :]
    logits = jnp.where(is_valid, scores + decay_bias, -jnp.inf)
    top_logit = jnp.maximum(jnp.max(logits, axis=3), own_score)
    weights = jnp.exp(logits - top_logit[..., None])
    own_weight = jnp.exp(own_score - top_logit)
    total_weight = jnp.sum(weights, axis=3) + own_weight
    cache_probs = (weights / total_weight[..., None]).astype(jnp.bfloat16)
    own_prob = (own_weight / total_weight).astype(jnp.bfloat16)
    mixed_heads = jnp.einsum(
        "sgrl,sgdl->sgrd", cache_probs, cache_value, preferred_element_type=jnp.float32
    )
    mixed_heads = (
        mixed_heads
        + own_prob.astype(jnp.float32)[..., None] * fresh_value.astype(jnp.float32)[:, :, None, :]
    )
    attn_heads = mixed_heads.reshape(seq_count, heads_local * head_size).astype(jnp.bfloat16)
    partial_value = jnp.dot(attn_heads, out_w, preferred_element_type=jnp.float32)
    attn_sum = lax.psum(partial_value.astype(jnp.bfloat16), "tp").astype(jnp.float32)
    resid_out = rounded(resid_in + attn_sum)
    post_norm = rms_scale(resid_out, post_gain.astype(jnp.float32)).astype(jnp.bfloat16)
    branch = jax.nn.sigmoid(jnp.dot(post_norm, branch_gate, preferred_element_type=jnp.float32))
    all_tokens = lax.all_gather(post_norm, "ep", axis=0, tiled=True)
    hidden = swiglu_rows(all_tokens, dense_gate_w, dense_up_w)
    squares = jnp.sum(hidden * hidden, axis=1)
    dense_terms = flat_terms(hidden, dense_down_w, ep_count, tp_count, seq_count)
    spread = jnp.broadcast_to(
        squares.reshape(ep_count, 1, seq_count), (ep_count, tp_count, seq_count)
    ).reshape(-1)
    dense_sum, square_sum = (
        lax.psum_scatter(
            dense_terms.reshape(-1, half_width), ("ep", "tp"), scatter_dimension=0, tiled=True
        ),
        lax.psum_scatter(spread, ("ep", "tp"), scatter_dimension=0, tiled=True),
    )
    dense_out = rounded(dense_sum * lax.rsqrt(square_sum / FF2 + norm_eps)[:, None])
    per_group = ep_count // GROUPS
    capacity = 2 * ((seq_count + 2 * per_group - 1) // (2 * per_group))
    route_count = expert_choice.shape[1]
    route_ids = expert_choice.reshape(-1)
    member = (route_ids[:, None] == jnp.arange(ep_count)[None, :]).astype(jnp.int32)
    slot_index = jnp.sum((jnp.cumsum(member, axis=0) - member) * member, axis=1)
    target = (route_ids * capacity + slot_index).reshape(seq_count, route_count)
    place_map = (target[:, :, None] == jnp.arange(ep_count * capacity)[None, None, :]).astype(
        jnp.bfloat16
    )
    outgoing = jnp.einsum("skc,sd->cd", place_map, post_norm, preferred_element_type=jnp.float32)
    outgoing = outgoing.astype(jnp.bfloat16).reshape(ep_count, capacity, model_width)
    arrived = lax.all_to_all(outgoing, "ep", split_axis=0, concat_axis=0, tiled=True)
    item_count = arrived.shape[1]
    slot_rows = arrived.reshape(-1, model_width)
    activated = swiglu_rows(slot_rows, expert_gate_w[0], expert_up_w[0]).astype(jnp.bfloat16)
    partial_out = jnp.dot(activated, expert_down_w[0], preferred_element_type=jnp.float32)
    partial_out = partial_out.reshape(ep_count, item_count, model_width)
    halves = lax.psum_scatter(
        partial_out.astype(jnp.bfloat16), "tp", scatter_dimension=2, tiled=True
    )
    returned = lax.all_to_all(halves, "ep", split_axis=0, concat_axis=0, tiled=True).reshape(
        ep_count * capacity, half_width
    )
    routed = jnp.einsum("skc,cd->skd", place_map, returned, preferred_element_type=jnp.float32)
    expert_sum = jnp.sum(route_weight[:, :, None] * routed, axis=1)
    resid_columns = lax.dynamic_slice_in_dim(resid_out, tp_rank * half_width, half_width, 1)
    mixed_out = (resid_columns + expert_sum + branch[:, None] * dense_out).astype(jnp.bfloat16)
    return (mixed_out, fresh_key, fresh_value, current)


def solution(mesh):
    placed = (
        P("ep", None),
        P(),
        P(None, "tp"),
        P(),
        P(),
        P(),
        P(),
        P(),
        P(),
        P("ep", "tp", None, None),
        P("ep", "tp", None, None),
        P("ep", "tp", None),
        P("ep"),
        P("tp", None),
        P(),
        P(),
        P(None, ("ep", "tp")),
        P(None, ("ep", "tp")),
        P(("ep", "tp"), None),
        P("ep", None),
        P("ep", None),
        P("ep", None, "tp"),
        P("ep", None, "tp"),
        P("ep", "tp", None),
    )
    return jax.shard_map(
        body,
        mesh=mesh,
        in_specs=placed,
        out_specs=(P("ep", "tp"), P("ep", "tp", None), P("ep", "tp", None), P("ep", "tp")),
        check_vma=False,
    )
```

profile of v0, /device:TPU:0, one launch (start us, length us, event | category | flops | bytes accessed | tf_op | source)
XLA Modules:
  0.0 239.2 jit_solution(11453295453262258375)
XLA Ops:
  7.3 0.8 broadcast_add_fusion
  8.1 0.9 iota_compare_fusion.1
  9.0 0.1 iota_compare_fusion
  9.0 1.3 select_reduce_fusion
  10.4 0.7 convert_element_type.95
  11.1 1.0 fusion.41
  12.2 1.2 fusion.68
  13.4 2.1 fusion.66
  15.5 0.1 reshape.187
  15.6 0.1 multiply_reduce_fusion.2
  15.8 1.3 fusion.63
  17.1 0.1 reshape.189
  17.2 0.1 multiply_reduce_fusion.3
  17.3 0.1 copy.61
  17.5 0.2 fusion.51
  17.7 1.9 fusion.69
  19.6 0.9 copy-done.1
  20.5 0.3 fusion.38
  20.8 0.2 convolution_convert_fusion.3
  21.0 0.1 reshape.192
  21.2 0.6 bitcast_convert_fusion
  21.8 3.1 %fusion.30 = bf16[24,8,64]{2,1,0:T(8,128)(2,1)S(1)} fusion(bf16[24,1,64,1024]{3,2,1,0:T(8,128)(2,1)} %param.34, f32[24,8,1024]{2,1,0:T(8,128)} %copy-done.1, f32[24,8]{1,0:T(8,128)S(1)} %get-tuple-element.9, f32[24,8]{1,0:T(8,128)S(1)} %multiply_maximum_fusion, f32[24,64]{1,0:T(8,128)S(1)} %get-tuple-element.4, f32[24,8]{1,0:T(8,128)S(1)} %get-tuple-element.8), kind=kOutput, calls=%fused_computation.24 | convolution fusion | flops 25792512 | bytes 3965184 | tf_op jit(solution)/shard_map/sgrl,sgdl->sgrd/dot_general | solution.py:115
  24.9 0.1 convert_element_type.106
  25.0 2.6 %convolution_convert_fusion.2 = bf16[24,2048]{1,0:T(8,128)(2,1)} fusion(bf16[24,512]{1,0:T(8,128)(2,1)S(1)} %convert_element_type.106, bf16[512,2048]{1,0:T(8,128)(2,1)} %param.37), kind=kOutput, calls=%fused_computation.6 | convolution fusion | flops 50380800 | bytes 2220032 | tf_op jit(solution)/shard_map/dot_general | solution.py:123
  27.7 20.6 %all-reduce.3.cloned.1.call-done = bf16[24,2048]{1,0:T(8,128)(2,1)} async-done(((bf16[24,2048]{1,0:T(8,128)(2,1)}), bf16[24,2048]{1,0:T(8,128)(2,1)}) %all-reduce.3.cloned.1.call-update) | async-done | bytes 98320 | tf_op jit(solution)/shard_map/psum | solution.py:124
  48.4 0.9 fusion.44
  49.3 0.1 multiply_reduce_fusion.1
  49.4 0.5 copy-done.4
  49.9 0.7 multiply_convert_fusion
  50.7 0.1 copy.64
  50.8 0.1 eq.42
  51.0 0.2 select_reduce_fusion.1
  51.2 0.1 reduce_sum.98
  51.3 0.1 copy.65
  51.4 0.1 convert_reduce_fusion
  51.5 1.2 fusion.71
  52.7 0.9 reshape.193
  53.6 24.4 %all_to_all.10 = bf16[16,6,2048]{2,1,0:T(8,128)(2,1)} all-to-all(bf16[16,6,2048]{2,1,0:T(8,128)(2,1)} %reshape.193), channel_id=1, replica_groups=mesh['ep'=16,'tp'=2] {'ep'}, dimensions={0} | all-to-all | bytes 786432 | tf_op jit(solution)/shard_map/all_to_all | solution.py:154
  78.1 1.2 reshape.194
  79.3 2.2 fusion.9
  81.5 1.1 fusion.24
  82.6 0.9 dot_general.64
  83.5 2.8 %convolution_convert_fusion = bf16[16,6,2048]{2,0,1:T(8,128)(2,1)} fusion(bf16[1,512,2048]{2,1,0:T(8,128)(2,1)} %param.47, bf16[16,6,512]{2,1,0:T(8,128)(2,1)S(1)} %dot_general.64), kind=kOutput, calls=%fused_computation.4 | convolution fusion | flops 201523200 | bytes 2588672 | tf_op jit(solution)/shard_map/dot_general | solution.py:158
  86.4 26.2 %all-gather.2.cloned.1.call-done = bf16[384,2048]{1,0:T(8,128)(2,1)} async-done(((bf16[24,2048]{1,0:T(8,128)(2,1)}), bf16[384,2048]{1,0:T(8,128)(2,1)}) %all-gather.2.cloned.1.call-update) | async-done | bytes 1572880 | tf_op jit(solution)/shard_map/all_gather | solution.py:128
  112.6 3.2 %fusion.70 = f32[384,512]{1,0:T(8,128)S(1)} fusion(bf16[384,2048]{1,0:T(8,128)(2,1)} %all-gather.2.cloned.1.call-done, bf16[2048,512]{1,0:T(8,128)(2,1)} %param.40), kind=kOutput, calls=%fused_computation.98 | convolution fusion | flops 805306368 | bytes 4456448 | tf_op jit(solution)/shard_map/dot_general | solution.py:21
  115.8 1.1 multiply_reduce_fusion
  117.0 0.4 copy-done.3
  117.4 2.7 %fusion.4 = f32[16,24,2,1024]{3,1,2,0:T(8,128)} fusion(bf16[16,24,512,1]{2,1,3,0:T(8,128)(2,1)S(1)} %bitcast.85, bf16[64,2,8,1024]{3,2,1,0:T(8,128)(2,1)S(1)} %bitcast.84), kind=kOutput, calls=%fused_computation.8 | convolution fusion | flops 805306368 | bytes 5636096 | tf_op jit(solution)/shard_map/esh,hcd->ecsd/dot_general | solution.py:29
  120.1 0.6 copy-done.9
  120.8 0.6 reduce-scatter.3.cloned.1.call-done
  121.4 1.8 copy.67
  123.1 6.8 %all-to-all-start.1 = ((bf16[16,6,1024]{2,1,0:T(8,128)(2,1)}), bf16[16,6,1024]{2,1,0:T(8,128)(2,1)S(1)}, u32[]{:S(2)}, u32[]{:S(2)}) async-start(bf16[16,6,1024]{2,1,0:T(8,128)(2,1)} %copy.67), calls=%async_computation.2 | async-start | bytes 524288 | tf_op jit(solution)/shard_map/all_to_all | solution.py:163
  129.9 0.7 fusion.49
  130.6 0.7 convert_element_type.110
  131.3 1.0 fusion.37
  132.3 7.9 %all-to-all-done.1 = bf16[16,6,1024]{2,1,0:T(8,128)(2,1)S(1)} async-done(((bf16[16,6,1024]{2,1,0:T(8,128)(2,1)}), bf16[16,6,1024]{2,1,0:T(8,128)(2,1)S(1)}, u32[]{:S(2)}, u32[]{:S(2)}) %all-to-all-start.1) | async-done | bytes 196640 | tf_op jit(solution)/shard_map/all_to_all | solution.py:163
  140.3 0.8 reshape.204
  141.0 1.2 fusion.23
  142.2 0.1 broadcast_in_dim.30
  142.3 0.1 reshape.199
  142.4 38.9 %all-reduce = f32[768]{0:T(1024)S(1)} all-reduce(f32[768]{0:T(1024)S(1)} %reshape.199), channel_id=4, replica_groups=mesh['ep'=16,'tp'=2] {'ep','tp'}, use_global_device_ids=true, to_apply=%region_15.16.clone | all-reduce | flops 768 | bytes 6144
  181.4 48.7 %reduce-scatter.5.cloned.1.call-done = f32[24,1024]{1,0:T(8,128)} async-done(((f32[768,1024]{1,0:T(8,128)}), f32[24,1024]{1,0:T(8,128)}) %reduce-scatter.5.cloned.1.call-update) | async-done | bytes 98320 | tf_op jit(solution)/shard_map/reduce_scatter | solution.py:136
  230.1 1.0 multiply_convert_fusion.1
  231.1 1.6 add_convert_fusion
  (68 shorter events, 1.0 us)
Async XLA Ops:
  7.2 10.6 %copy-start = (bf16[24,1,64,1024]{3,2,1,0:T(8,128)(2,1)S(1)}, bf16[24,1,64,1024]{3,2,1,0:T(8,128)(2,1)}, u32[]{:S(2)}) copy-start(bf16[24,1,64,1024]{3,2,1,0:T(8,128)(2,1)} %param.33) | copy-start | bytes 9437188
  7.2 8.6 %copy-start.2 = (bf16[24,2048]{1,0:T(8,128)(2,1)S(1)}, bf16[24,2048]{1,0:T(8,128)(2,1)}, u32[]{:S(2)}) copy-start(bf16[24,2048]{1,0:T(8,128)(2,1)} %param.24) | copy-start | bytes 294916
  7.2 8.4 %copy-start.19 = (bf16[64]{0:T(256)(128)(2,1)S(1)}, bf16[64]{0:T(256)(128)(2,1)}, u32[]{:S(2)}) copy-start(bf16[64]{0:T(256)(128)(2,1)} %param.31) | copy-start | bytes 388
  7.2 8.5 %copy-start.20 = (bf16[64]{0:T(256)(128)(2,1)S(1)}, bf16[64]{0:T(256)(128)(2,1)}, u32[]{:S(2)}) copy-start(bf16[64]{0:T(256)(128)(2,1)} %param.32) | copy-start | bytes 388
  7.2 41.1 %all-reduce.3.cloned.1.call-start = ((), (), s32[]{:S(2)}) async-start(), calls=%async_computation.4 | async-start | bytes 196608 | tf_op jit(solution)/shard_map/psum | solution.py:124
  13.4 6.3 %copy-start.7 = (f32[24,8]{0,1:T(8,128)}, f32[24,8]{0,1:T(8,128)S(1)}, u32[]{:S(2)}) copy-start(f32[24,8]{0,1:T(8,128)S(1)} %fusion.55) | copy-start | bytes 2308
  15.8 3.8 %copy-start.11 = (f32[64]{0:T(128)}, f32[64]{0:T(128)S(1)}, u32[]{:S(2)}) copy-start(f32[64]{0:T(128)S(1)} %convert_element_type.99) | copy-start | bytes 772
  17.4 2.2 copy-start.13
  17.7 3.1 %copy-start.6 = (bf16[2048,128]{1,0:T(8,128)(2,1)S(1)}, bf16[2048,128]{1,0:T(8,128)(2,1)}, u32[]{:S(2)}) copy-start(bf16[2048,128]{1,0:T(8,128)(2,1)} %param.28) | copy-start | bytes 1572868
  19.6 0.9 copy-start.1
  24.9 2.8 %copy-start.8 = (bf16[2048]{0:T(1024)(128)(2,1)S(1)}, bf16[2048]{0:T(1024)(128)(2,1)}, u32[]{:S(2)}) copy-start(bf16[2048]{0:T(1024)(128)(2,1)} %param.38) | copy-start | bytes 12292
  24.9 25.8 %copy-start.10 = (s32[24,2]{0,1:T(2,128)S(1)}, s32[24,2]{0,1:T(2,128)}, u32[]{:S(2)}) copy-start(s32[24,2]{0,1:T(2,128)} %param.43) | copy-start | bytes 580
  27.6 84.9 %all-gather.2.cloned.1.call-start = ((), (), s32[]{:S(2)}) async-start(), calls=%async_computation.6 | async-start | bytes 1671168 | tf_op jit(solution)/shard_map/all_gather | solution.py:128
  49.3 0.6 copy-start.4
  50.6 70.7 %reduce-scatter.3.cloned.1.call-start = ((), (), s32[]{:S(2)}) async-start(), calls=%async_computation.5 | async-start | bytes 589824 | tf_op jit(solution)/shard_map/reduce_scatter | solution.py:160
  79.2 2.2 copy-start.16
  86.4 143.8 %reduce-scatter.5.cloned.1.call-start = ((), (), s32[]{:S(2)}) async-start(), calls=%async_computation.7 | async-start | bytes 3244032 | tf_op jit(solution)/shard_map/reduce_scatter | solution.py:136
  112.6 3.2 %copy-start.17 = (bf16[2048,512]{1,0:T(8,128)(2,1)S(1)}, bf16[2048,512]{1,0:T(8,128)(2,1)}, u32[]{:S(2)}) copy-start(bf16[2048,512]{1,0:T(8,128)(2,1)} %param.41) | copy-start | bytes 6291460
  112.6 3.2 %copy-start.18 = (bf16[384,2048]{1,0:T(8,128)(2,1)S(1)}, bf16[384,2048]{1,0:T(8,128)(2,1)}, u32[]{:S(2)}) copy-start(bf16[384,2048]{1,0:T(8,128)(2,1)} %all-gather.2.cloned.1.call-done) | copy-start | bytes 4718596
  115.8 1.6 copy-start.3
  120.1 0.7 copy-start.9
  120.1 9.9 %copy-start.12 = (f32[64]{0:T(128)S(1)}, f32[64]{0:T(128)}, u32[]{:S(2)}) copy-start(f32[64]{0:T(128)} %copy-done.11) | copy-start | bytes 772
  120.1 9.9 %copy-start.14 = (f32[24,1]{0,1:T(1,128)S(1)}, f32[24,1]{0,1:T(1,128)}, u32[]{:S(2)}) copy-start(f32[24,1]{0,1:T(1,128)} %copy-done.13) | copy-start | bytes 292
  120.1 10.5 %copy-start.5 = (bf16[24,2048]{1,0:T(8,128)(2,1)S(1)}, bf16[24,2048]{1,0:T(8,128)(2,1)}, u32[]{:S(2)}) copy-start(bf16[24,2048]{1,0:T(8,128)(2,1)} %copy-done.4) | copy-start | bytes 294916
  120.1 21.0 %copy-start.15 = (f32[24,2]{0,1:T(2,128)S(1)}, f32[24,2]{0,1:T(2,128)}, u32[]{:S(2)}) copy-start(f32[24,2]{0,1:T(2,128)} %param.44) | copy-start | bytes 580
  123.1 17.1 %all-to-all-start.1 = ((bf16[16,6,1024]{2,1,0:T(8,128)(2,1)}), bf16[16,6,1024]{2,1,0:T(8,128)(2,1)S(1)}, u32[]{:S(2)}, u32[]{:S(2)}) async-start(bf16[16,6,1024]{2,1,0:T(8,128)(2,1)} %copy.67), calls=%async_computation.2 | async-start | bytes 524288 | tf_op jit(solution)/shard_map/all_to_all | solution.py:163
Sparse Core Ops, SparseCore 0:
  27.8 20.5 all-reduce.2
  51.1 61.4 all-gather.1
  114.8 6.5 reduce-scatter.2
  126.7 103.4 reduce-scatter.4
where the time goes:
time: 240 us; the launch traced here: 239 us
  waiting for transfers between devices  104 us (43%)
  blocking collectives  63.3 us (26%)
  matrix products  29.1 us (12%)
  between operations  14.2 us (6%)
  other arithmetic  12.2 us (5%)
  local copies, waits for them, and re-layouts  9.26 us (4%)
  starting transfers between devices  6.92 us (3%)
    reduce_scatter x1, waiting for transfers between devices, body(): lax.psum_scatter(dense_terms.reshape(-1, half_width), ('ep', 'tp'), scatt...  48.7 us
    unnamed x1, blocking collectives  38.9 us
    all_gather x1, waiting for transfers between devices, body(): all_tokens = lax.all_gather(post_norm, 'ep', axis=0, tiled=True)  26.2 us
    all_to_all x1, blocking collectives, body(): lax.all_to_all(outgoing, 'ep', split_axis=0, concat_axis=0, tiled=True)  24.4 us
    psum x1, waiting for transfers between devices, body(): lax.psum(partial_value.astype(jnp.bfloat16), 'tp').astype(jnp.float32)  20.6 us
    all_to_all x1, waiting for transfers between devices, body(): lax.all_to_all(halves, 'ep', split_axis=0, concat_axis=0, tiled=True)  7.95 us
    all_to_all x1, starting transfers between devices, body(): lax.all_to_all(halves, 'ep', split_axis=0, concat_axis=0, tiled=True)  6.76 us
    dot_general x2, matrix products, swiglu_rows(): jnp.dot(inputs, gate_weight, preferred_element_type=jnp.float32)  5.38 us
  transfers between devices with their start and end apart: 5, of which 5 were waited for; matrix products, arithmetic and copies ran while one was open for 10% of the time, Pallas kernels for 0%

commit v1 on v0

--- a/solution.py
+++ b/solution.py
@@ -1,3 +1,4 @@
+import functools
 import jax
 import jax.numpy as jnp
 from jax import lax
@@ -6,6 +7,14 @@
 FF2 = 16384
 GROUPS = 4
 norm_eps = 1e-06
+
+
+def numbers_hold(message, device_axis):
+    mixed_arr = jnp.sum(lax.all_gather(message, axis_name=device_axis), 0)
+    return mixed_arr
+
+
+report_slots_in = functools.partial(numbers_hold, device_axis="tp")
 
 
 def rms_scale(values, gain_vec):
@@ -121,7 +130,7 @@
     )
     attn_heads = mixed_heads.reshape(seq_count, heads_local * head_size).astype(jnp.bfloat16)
     partial_value = jnp.dot(attn_heads, out_w, preferred_element_type=jnp.float32)
-    attn_sum = lax.psum(partial_value.astype(jnp.bfloat16), "tp").astype(jnp.float32)
+    attn_sum = report_slots_in(partial_value.astype(jnp.bfloat16)).astype(jnp.float32)
     resid_out = rounded(resid_in + attn_sum)
     post_norm = rms_scale(resid_out, post_gain.astype(jnp.float32)).astype(jnp.bfloat16)
     branch = jax.nn.sigmoid(jnp.dot(post_norm, branch_gate, preferred_element_type=jnp.float32))

time: 240 us -> 216 us (0.900)
  waiting for transfers between devices: 104 us -> 77.8 us
  blocking collectives: 63.3 us -> 66.1 us
  starting transfers between devices: 6.92 us -> 4.46 us
    psum x1 -> x0, waiting for transfers between devices: 20.6 us -> none  [body(): lax.psum(partial_value.astype(jnp.bfloat16), 'tp').astype(jnp.float32)]
    reduce_scatter x1, waiting for transfers between devices: 48.7 us -> 44.4 us  [body(): lax.psum_scatter(dense_terms.reshape(-1, half_width), ('ep', 'tp'), scatt...]
    all_to_all x1, starting transfers between devices: 6.76 us -> 4.33 us  [body(): lax.all_to_all(halves, 'ep', split_axis=0, concat_axis=0, tiled=True)]
  transfers between devices with their start and end apart: 5 -> 4, of which waited for: 5 -> 3; matrix products, arithmetic and copies ran while one was open for 10% -> 11% of each run, Pallas kernels for 0% -> 0%
where the time goes in v1:
time: 216 us; the launch traced here: 215 us
  waiting for transfers between devices  77.8 us (36%)
  blocking collectives  66.1 us (31%)
  matrix products  27.5 us (13%)
  between operations  16 us (7%)
  other arithmetic  14 us (6%)
  local copies, waits for them, and re-layouts  9.46 us (4%)
  starting transfers between devices  4.46 us (2%)
    reduce_scatter x1, waiting for transfers between devices, body(): lax.psum_scatter(dense_terms.reshape(-1, half_width), ('ep', 'tp'), scatt...  44.4 us
    unnamed x1, blocking collectives  38.7 us
    all_gather x1, waiting for transfers between devices, body(): all_tokens = lax.all_gather(post_norm, 'ep', axis=0, tiled=True)  25.6 us
    all_to_all x1, blocking collectives, body(): lax.all_to_all(outgoing, 'ep', split_axis=0, concat_axis=0, tiled=True)  25.3 us
    all_to_all x1, waiting for transfers between devices, body(): lax.all_to_all(halves, 'ep', split_axis=0, concat_axis=0, tiled=True)  7.67 us
    dot_general x2, matrix products, swiglu_rows(): jnp.dot(inputs, gate_weight, preferred_element_type=jnp.float32)  5.38 us
    all_to_all x1, starting transfers between devices, body(): lax.all_to_all(halves, 'ep', split_axis=0, concat_axis=0, tiled=True)  4.33 us
  transfers between devices with their start and end apart: 4, of which 3 were waited for; matrix products, arithmetic and copies ran while one was open for 11% of the time, Pallas kernels for 0%

profile of v1, /device:TPU:0, one launch (start us, length us, event | category | flops | bytes accessed | tf_op | source)
XLA Modules:
  0.0 215.2 jit_solution(17143496430903450395)
XLA Ops:
  8.1 0.8 broadcast_add_fusion
  8.9 0.9 iota_compare_fusion.1
  9.8 1.3 convert_element_type.116
  11.1 0.1 iota_compare_fusion
  11.2 1.3 select_reduce_fusion
  12.6 0.7 convert_element_type.97
  13.3 1.0 fusion.41
  14.3 1.2 fusion.68
  15.6 2.1 fusion.66
  17.6 0.1 reshape.187
  17.7 0.1 multiply_reduce_fusion.2
  17.9 1.3 fusion.63
  19.2 0.1 reshape.189
  19.3 0.1 multiply_reduce_fusion.3
  19.4 0.1 copy.61
  19.6 0.2 fusion.51
  19.9 1.9 fusion.69
  21.8 0.9 copy-done.1
  22.6 0.3 fusion.38
  22.9 0.2 convolution_convert_fusion.3
  23.2 0.1 reshape.192
  23.3 0.6 bitcast_convert_fusion
  23.9 3.1 %fusion.30 = bf16[24,8,64]{2,1,0:T(8,128)(2,1)S(1)} fusion(bf16[24,1,64,1024]{3,2,1,0:T(8,128)(2,1)} %param.34, f32[24,8,1024]{2,1,0:T(8,128)} %copy-done.1, f32[24,8]{1,0:T(8,128)S(1)} %get-tuple-element.9, f32[24,8]{1,0:T(8,128)S(1)} %multiply_maximum_fusion, f32[24,64]{1,0:T(8,128)S(1)} %get-tuple-element.4, f32[24,8]{1,0:T(8,128)S(1)} %get-tuple-element.8), kind=kOutput, calls=%fused_computation.24 | convolution fusion | flops 25792512 | bytes 3965184 | tf_op jit(solution)/shard_map/sgrl,sgdl->sgrd/dot_general | solution.py:124
  27.0 0.1 convert_element_type.108
  27.1 2.0 convolution_convert_fusion.2
  29.1 2.1 all-gather
  31.3 0.1 multiply_reduce_fusion.1
  31.4 0.5 copy-done.4
  31.9 1.4 multiply_convert_fusion
  33.4 0.1 copy.64
  33.5 0.1 eq.42
  33.6 0.1 reduce_window_sum.11
  33.7 0.2 select_reduce_fusion.1
  33.9 0.1 reduce_sum.111
  34.0 0.1 copy.65
  34.1 0.7 multiply_add_fusion
  34.9 1.2 fusion.71
  36.0 0.9 reshape.193
  37.0 25.3 %all_to_all.10 = bf16[16,6,2048]{2,1,0:T(8,128)(2,1)} all-to-all(bf16[16,6,2048]{2,1,0:T(8,128)(2,1)} %reshape.193), channel_id=1, replica_groups=mesh['ep'=16,'tp'=2] {'ep'}, dimensions={0} | all-to-all | bytes 786432 | tf_op jit(solution)/shard_map/all_to_all | solution.py:163
  62.3 1.2 reshape.194
  63.4 2.2 %fusion.9 = f32[96,512]{1,0:T(8,128)S(1)} fusion(bf16[96,2048]{1,0:T(8,128)(2,1)S(1)} %reshape.194, bf16[1,2048,512]{2,1,0:T(8,128)(2,1)} %param.45), kind=kOutput, calls=%fused_computation.13 | convolution fusion | flops 201326592 | bytes 2686976 | tf_op jit(solution)/shard_map/dot_general | solution.py:30
  65.7 1.1 fusion.24
  66.8 0.9 dot_general.64
  67.7 2.8 %convolution_convert_fusion = bf16[16,6,2048]{2,0,1:T(8,128)(2,1)} fusion(bf16[1,512,2048]{2,1,0:T(8,128)(2,1)} %param.47, bf16[16,6,512]{2,1,0:T(8,128)(2,1)S(1)} %dot_general.64), kind=kOutput, calls=%fused_computation.4 | convolution fusion | flops 201523200 | bytes 2588672 | tf_op jit(solution)/shard_map/dot_general | solution.py:167
  70.6 25.6 %all-gather.3.cloned.1.call-done = bf16[384,2048]{1,0:T(8,128)(2,1)} async-done(((bf16[24,2048]{1,0:T(8,128)(2,1)}), bf16[384,2048]{1,0:T(8,128)(2,1)}) %all-gather.3.cloned.1.call-update) | async-done | bytes 1572880 | tf_op jit(solution)/shard_map/all_gather | solution.py:137
  96.2 3.2 %fusion.70 = f32[384,512]{1,0:T(8,128)S(1)} fusion(bf16[384,2048]{1,0:T(8,128)(2,1)} %all-gather.3.cloned.1.call-done, bf16[2048,512]{1,0:T(8,128)(2,1)} %param.40), kind=kOutput, calls=%fused_computation.98 | convolution fusion | flops 805306368 | bytes 4456448 | tf_op jit(solution)/shard_map/dot_general | solution.py:30
  99.4 1.1 multiply_reduce_fusion
  100.6 0.4 copy-done.3
  101.0 2.7 %fusion.4 = f32[16,24,2,1024]{3,1,2,0:T(8,128)} fusion(bf16[16,24,512,1]{2,1,3,0:T(8,128)(2,1)S(1)} %bitcast.87, bf16[64,2,8,1024]{3,2,1,0:T(8,128)(2,1)S(1)} %bitcast.85), kind=kOutput, calls=%fused_computation.8 | convolution fusion | flops 805306368 | bytes 5636096 | tf_op jit(solution)/shard_map/esh,hcd->ecsd/dot_general | solution.py:38
  103.7 0.8 copy-done.5
  104.6 0.7 convert_element_type.112
  105.3 1.8 copy.67
  107.1 4.3 %all-to-all-start.1 = ((bf16[16,6,1024]{2,1,0:T(8,128)(2,1)}), bf16[16,6,1024]{2,1,0:T(8,128)(2,1)S(1)}, u32[]{:S(2)}, u32[]{:S(2)}) async-start(bf16[16,6,1024]{2,1,0:T(8,128)(2,1)} %copy.67), calls=%async_computation.2 | async-start | bytes 524288 | tf_op jit(solution)/shard_map/all_to_all | solution.py:172
  111.4 0.7 fusion.49
  112.1 0.1 fusion.37
  112.2 7.7 %all-to-all-done.1 = bf16[16,6,1024]{2,1,0:T(8,128)(2,1)S(1)} async-done(((bf16[16,6,1024]{2,1,0:T(8,128)(2,1)}), bf16[16,6,1024]{2,1,0:T(8,128)(2,1)S(1)}, u32[]{:S(2)}, u32[]{:S(2)}) %all-to-all-start.1) | async-done | bytes 196640 | tf_op jit(solution)/shard_map/all_to_all | solution.py:172
  119.9 0.8 reshape.205
  120.7 1.2 fusion.23
  121.8 0.1 broadcast_in_dim.30
  121.9 0.1 reshape.199
  122.0 38.7 %all-reduce = f32[768]{0:T(1024)S(1)} all-reduce(f32[768]{0:T(1024)S(1)} %reshape.199), channel_id=5, replica_groups=mesh['ep'=16,'tp'=2] {'ep','tp'}, use_global_device_ids=true, to_apply=%region_15.16.clone | all-reduce | flops 768 | bytes 6144
  160.8 44.4 %reduce-scatter.5.cloned.1.call-done = f32[24,1024]{1,0:T(8,128)} async-done(((f32[768,1024]{1,0:T(8,128)}), f32[24,1024]{1,0:T(8,128)}) %reduce-scatter.5.cloned.1.call-update) | async-done | bytes 98320 | tf_op jit(solution)/shard_map/reduce_scatter | solution.py:145
  205.2 1.0 multiply_convert_fusion.1
  206.2 1.6 add_convert_fusion
  (67 shorter events, 1.0 us)
Async XLA Ops:
  8.0 11.8 %copy-start = (bf16[24,1,64,1024]{3,2,1,0:T(8,128)(2,1)S(1)}, bf16[24,1,64,1024]{3,2,1,0:T(8,128)(2,1)}, u32[]{:S(2)}) copy-start(bf16[24,1,64,1024]{3,2,1,0:T(8,128)(2,1)} %param.33) | copy-start | bytes 9437188
  8.0 9.9 %copy-start.2 = (bf16[24,2048]{1,0:T(8,128)(2,1)S(1)}, bf16[24,2048]{1,0:T(8,128)(2,1)}, u32[]{:S(2)}) copy-start(bf16[24,2048]{1,0:T(8,128)(2,1)} %param.24) | copy-start | bytes 294916
  8.0 9.7 %copy-start.19 = (bf16[64]{0:T(256)(128)(2,1)S(1)}, bf16[64]{0:T(256)(128)(2,1)}, u32[]{:S(2)}) copy-start(bf16[64]{0:T(256)(128)(2,1)} %param.31) | copy-start | bytes 388
  8.0 9.8 %copy-start.20 = (bf16[64]{0:T(256)(128)(2,1)S(1)}, bf16[64]{0:T(256)(128)(2,1)}, u32[]{:S(2)}) copy-start(bf16[64]{0:T(256)(128)(2,1)} %param.32) | copy-start | bytes 388
  8.0 88.2 %all-gather.3.cloned.1.call-start = ((), (), s32[]{:S(2)}) async-start(), calls=%async_computation.5 | async-start | bytes 1671168 | tf_op jit(solution)/shard_map/all_gather | solution.py:137
  15.5 6.3 %copy-start.8 = (f32[24,8]{0,1:T(8,128)}, f32[24,8]{0,1:T(8,128)S(1)}, u32[]{:S(2)}) copy-start(f32[24,8]{0,1:T(8,128)S(1)} %fusion.55) | copy-start | bytes 2308
  17.9 3.8 %copy-start.11 = (f32[64]{0:T(128)}, f32[64]{0:T(128)S(1)}, u32[]{:S(2)}) copy-start(f32[64]{0:T(128)S(1)} %convert_element_type.101) | copy-start | bytes 772
  19.5 2.2 %copy-start.13 = (f32[24,1]{0,1:T(1,128)}, f32[24,1]{0,1:T(1,128)S(1)}, u32[]{:S(2)}) copy-start(f32[24,1]{0,1:T(1,128)S(1)} %constant_dynamic-slice_fusion.2) | copy-start | bytes 292
  19.8 3.1 %copy-start.7 = (bf16[2048,128]{1,0:T(8,128)(2,1)S(1)}, bf16[2048,128]{1,0:T(8,128)(2,1)}, u32[]{:S(2)}) copy-start(bf16[2048,128]{1,0:T(8,128)(2,1)} %param.28) | copy-start | bytes 1572868
  21.7 0.9 copy-start.1
  27.0 6.4 %copy-start.10 = (s32[24,2]{0,1:T(2,128)S(1)}, s32[24,2]{0,1:T(2,128)}, u32[]{:S(2)}) copy-start(s32[24,2]{0,1:T(2,128)} %param.43) | copy-start | bytes 580
  31.2 0.6 copy-start.4
  33.3 72.0 %reduce-scatter.3.cloned.1.call-start = ((), (), s32[]{:S(2)}) async-start(), calls=%async_computation.4 | async-start | bytes 589824 | tf_op jit(solution)/shard_map/reduce_scatter | solution.py:169
  63.4 2.2 %copy-start.16 = (bf16[1,2048,512]{2,1,0:T(8,128)(2,1)S(1)}, bf16[1,2048,512]{2,1,0:T(8,128)(2,1)}, u32[]{:S(2)}) copy-start(bf16[1,2048,512]{2,1,0:T(8,128)(2,1)} %param.46) | copy-start | bytes 6291460
  70.5 134.7 %reduce-scatter.5.cloned.1.call-start = ((), (), s32[]{:S(2)}) async-start(), calls=%async_computation.6 | async-start | bytes 3244032 | tf_op jit(solution)/shard_map/reduce_scatter | solution.py:145
  96.2 3.2 %copy-start.17 = (bf16[2048,512]{1,0:T(8,128)(2,1)S(1)}, bf16[2048,512]{1,0:T(8,128)(2,1)}, u32[]{:S(2)}) copy-start(bf16[2048,512]{1,0:T(8,128)(2,1)} %param.41) | copy-start | bytes 6291460
  96.2 3.2 %copy-start.18 = (bf16[384,2048]{1,0:T(8,128)(2,1)S(1)}, bf16[384,2048]{1,0:T(8,128)(2,1)}, u32[]{:S(2)}) copy-start(bf16[384,2048]{1,0:T(8,128)(2,1)} %all-gather.3.cloned.1.call-done) | copy-start | bytes 4718596
  99.4 1.6 copy-start.3
  103.7 0.9 copy-start.5
  103.7 1.6 copy-start.9
  103.7 7.7 %copy-start.12 = (f32[64]{0:T(128)S(1)}, f32[64]{0:T(128)}, u32[]{:S(2)}) copy-start(f32[64]{0:T(128)} %copy-done.11) | copy-start | bytes 772
  103.7 7.7 %copy-start.14 = (f32[24,1]{0,1:T(1,128)S(1)}, f32[24,1]{0,1:T(1,128)}, u32[]{:S(2)}) copy-start(f32[24,1]{0,1:T(1,128)} %copy-done.13) | copy-start | bytes 292
  103.7 8.4 %copy-start.6 = (bf16[24,2048]{1,0:T(8,128)(2,1)S(1)}, bf16[24,2048]{1,0:T(8,128)(2,1)}, u32[]{:S(2)}) copy-start(bf16[24,2048]{1,0:T(8,128)(2,1)} %multiply_convert_fusion) | copy-start | bytes 294916
  103.7 17.0 %copy-start.15 = (f32[24,2]{0,1:T(2,128)S(1)}, f32[24,2]{0,1:T(2,128)}, u32[]{:S(2)}) copy-start(f32[24,2]{0,1:T(2,128)} %param.44) | copy-start | bytes 580
  107.1 12.8 %all-to-all-start.1 = ((bf16[16,6,1024]{2,1,0:T(8,128)(2,1)}), bf16[16,6,1024]{2,1,0:T(8,128)(2,1)S(1)}, u32[]{:S(2)}, u32[]{:S(2)}) async-start(bf16[16,6,1024]{2,1,0:T(8,128)(2,1)} %copy.67), calls=%async_computation.2 | async-start | bytes 524288 | tf_op jit(solution)/shard_map/all_to_all | solution.py:172
Sparse Core Ops, SparseCore 0:
  33.4 62.7 all-gather.2
Sparse Core Ops, SparseCore 1:
  70.6 6.5 reduce-scatter.2
  103.8 101.4 reduce-scatter.4
